TPU v7x, 32 devices: a whole 2x2x4 slice. The times are simulated.
32 devices in a mesh: fs: 8 (over z, x), tp: 4 (over y, core).
Axes of the slice: x: 2, y: 2, z: 4, core: 2. Of those that a mesh axis runs over, the one named last changes fastest.
Arguments:
- weights: float32 [2, 5632, 2048], P(None, 'fs', 'tp'), may hold values from -6 to 6
- momentum: float32 [2, 5632, 2048], P(None, 'fs', 'tp'), may hold values from -12 to 12
- gradients: float32 [2, 5632, 2048], P(None, 'fs', 'tp'), may hold values from -140 to 140
Outputs:
- new_weights: float32 [2, 5632, 2048], P(None, 'fs', 'tp')
- new_momentum: float32 [2, 5632, 2048], P(None, 'fs', 'tp')
- update: float32 [2, 5632, 2048], P(None, 'fs', 'tp')
All inputs are finite; a program needn't handle non-finite values.
Results may differ from a plain program's by a relative error of at most 0.035.
Values may be sent and summed in bfloat16 or wider, within the bound.
A program may use at most 64 MiB of HBM per device.

v0:
```python
import math

import jax
import jax.numpy as jnp
from jax import lax
from jax.sharding import PartitionSpec as P

D = 2048
FF = 5632
ITERS = 3


MOMENTUM_DECAY = 0.95
FIRST_COEF = 3.4445
SECOND_COEF = -4.775
THIRD_COEF = 2.0315
LEARN_RATE = 0.02
WEIGHT_DECAY = 0.1
EPSILON = 1e-07
STEP_SCALE = 0.2
NORM_SAFETY = 1.8


def per_device(weights, momentum, gradients):
    new_momentum = MOMENTUM_DECAY * momentum + gradients
    iterate = gradients + MOMENTUM_DECAY * new_momentum
    for step in range(ITERS):
        plain = iterate.astype(jnp.bfloat16)
        row_whole = lax.all_gather(plain, "tp", axis=2, tiled=True)
        partial_value = jnp.einsum(
            "prj,prk->pjk", plain, row_whole, preferred_element_type=jnp.float32
        )
        gram_share = lax.psum_scatter(partial_value, "fs", scatter_dimension=2, tiled=True)
        if step == 0:
            squares = lax.psum(jnp.sum(gram_share * gram_share, axis=(1, 2)), ("fs", "tp"))
        gram_bf = lax.all_gather(gram_share.astype(jnp.bfloat16), "fs", axis=2, tiled=True)
        if step == 0:
            ratio = (1.0 / (NORM_SAFETY * jnp.sqrt(jnp.sqrt(squares / D)) + EPSILON))[:, None, None]
        else:
            ratio = 1.0
        cubed = jnp.einsum("prk,pjk->prj", row_whole, gram_bf, preferred_element_type=jnp.float32)
        cubed = (cubed * ratio**3).astype(jnp.bfloat16)
        folded = jnp.einsum(
            "prk,pjk->prj",
            lax.all_gather(cubed, "tp", axis=2, tiled=True),
            gram_bf,
            preferred_element_type=jnp.float32,
        )
        iterate = (
            FIRST_COEF * ratio * iterate
            + SECOND_COEF * cubed.astype(jnp.float32)
            + THIRD_COEF * (ratio * ratio) * folded
        )
    update = STEP_SCALE * math.sqrt(max(FF, D)) * iterate
    new_weights = weights * (1.0 - LEARN_RATE * WEIGHT_DECAY) - LEARN_RATE * update
    return (new_weights, new_momentum, update)


def solution(mesh):
    in_specs = (P(None, "fs", "tp"), P(None, "fs", "tp"), P(None, "fs", "tp"))
    out_specs = (P(None, "fs", "tp"), P(None, "fs", "tp"), P(None, "fs", "tp"))
    return jax.shard_map(
        per_device, mesh=mesh, in_specs=in_specs, out_specs=out_specs, check_vma=False
    )
```

profile of v0, /device:TPU:0, one launch (start us, length us, event | category | flops | bytes accessed | tf_op | source)
XLA Modules:
  0.0 1039.8 jit_solution(2336283370231378505)
XLA Ops:
  7.2 0.0 all-gather.10.cloned.1.call-start
  7.2 5.5 fusion
  12.7 0.0 all-gather.10.cloned.1.call-update
  12.7 0.0 reduce-scatter.4.cloned.1.call-start
  12.8 46.2 %all-gather.10.cloned.1.call-done = bf16[2,704,2048]{2,1,0:T(8,128)(2,1)} async-done(((bf16[2,704,512]{2,1,0:T(8,128)(2,1)}), bf16[2,704,2048]{2,1,0:T(8,128)(2,1)}) %all-gather.10.cloned.1.call-update) | async-done | bytes 5767184 | tf_op jit(solution)/shard_map/all_gather | solution.py:29
  59.0 9.9 fusion.3
  68.9 0.0 reduce-scatter.4.cloned.1.call-update
  68.9 0.0 all-gather.12.cloned.1.call-start
  69.0 147.9 %reduce-scatter.4.cloned.1.call-done = f32[2,512,256]{2,1,0:T(8,128)} async-done(((f32[2,512,2048]{2,1,0:T(8,128)}), f32[2,512,256]{2,1,0:T(8,128)}) %reduce-scatter.4.cloned.1.call-update) | async-done | bytes 1048592 | tf_op jit(solution)/shard_map/reduce_scatter | solution.py:33
  216.9 2.5 multiply_reduce_fusion
  219.4 0.0 all-gather.12.cloned.1.call-update
  219.5 0.0 all-gather.14.cloned.1.call-start
  219.5 42.7 %psum.7 = f32[2]{0:T(128)S(1)} all-reduce(f32[2]{0:T(128)S(1)} %get-tuple-element.9), channel_id=1, replica_groups=mesh['fs'=8,'tp'=4] {'fs','tp'}, use_global_device_ids=true, to_apply=%region_2.0 | all-reduce | flops 2 | bytes 16 | tf_op jit(solution)/shard_map/psum | solution.py:35
  262.2 33.0 %all-gather.12.cloned.1.call-done = bf16[2,512,2048]{2,1,0:T(8,128)(2,1)} async-done(((bf16[2,512,256]{2,1,0:T(8,128)(2,1)}), bf16[2,512,2048]{2,1,0:T(8,128)(2,1)}) %all-gather.12.cloned.1.call-update) | async-done | bytes 4194320 | tf_op jit(solution)/shard_map/all_gather | solution.py:36
  295.3 8.3 multiply_convert_fusion
  303.6 0.0 all-gather.14.cloned.1.call-update
  303.6 0.0 all-gather.16.cloned.1.call-start
  303.6 41.7 %all-gather.14.cloned.1.call-done = bf16[2,704,2048]{2,1,0:T(8,128)(2,1)} async-done(((bf16[2,704,512]{2,1,0:T(8,128)(2,1)}), bf16[2,704,2048]{2,1,0:T(8,128)(2,1)}) %all-gather.14.cloned.1.call-update) | async-done | bytes 5767184 | tf_op jit(solution)/shard_map/all_gather | solution.py:45
  345.3 10.7 %fusion.1 = (bf16[2,704,512]{2,1,0:T(8,128)(2,1)}, f32[2,704,512]{2,1,0:T(8,128)}) fusion(bf16[2,704,2048]{2,1,0:T(8,128)(2,1)} %all-gather.14.cloned.1.call-done, bf16[2,512,2048]{2,1,0:T(8,128)(2,1)} %all-gather.12.cloned.1.call-done, f32[2]{0:T(128)S(1)} %get-tuple-element.11, bf16[2,704,512]{2,1,0:T(8,128)(2,1)} %multiply_convert_fusion, ...), kind=kOutput, calls=%fused_computation.16 | convolution fusion | flops 2959278080 | bytes 21495824 | tf_op jit(solution)/shard_map/prk,pjk->prj/dot_general | solution.py:43
  356.0 0.0 all-gather.16.cloned.1.call-update
  356.0 0.2 reduce-scatter.6.cloned.1.call-start
  356.3 43.3 %all-gather.16.cloned.1.call-done = bf16[2,704,2048]{2,1,0:T(8,128)(2,1)} async-done(((bf16[2,704,512]{2,1,0:T(8,128)(2,1)}), bf16[2,704,2048]{2,1,0:T(8,128)(2,1)}) %all-gather.16.cloned.1.call-update) | async-done | bytes 5767184 | tf_op jit(solution)/shard_map/all_gather | solution.py:29
  399.6 9.9 fusion.4
  409.5 0.0 reduce-scatter.6.cloned.1.call-update
  409.5 0.0 all-gather.18.cloned.1.call-start
  409.5 147.9 %reduce-scatter.6.cloned.1.call-done = f32[2,512,256]{2,1,0:T(8,128)} async-done(((f32[2,512,2048]{2,1,0:T(8,128)}), f32[2,512,256]{2,1,0:T(8,128)}) %reduce-scatter.6.cloned.1.call-update) | async-done | bytes 1048592 | tf_op jit(solution)/shard_map/reduce_scatter | solution.py:33
  557.5 2.1 convert_element_type.41
  559.6 0.0 all-gather.18.cloned.1.call-update
  559.6 0.0 all-gather.20.cloned.1.call-start
  559.6 74.2 %all-gather.18.cloned.1.call-done = bf16[2,512,2048]{2,1,0:T(8,128)(2,1)} async-done(((bf16[2,512,256]{2,1,0:T(8,128)(2,1)}), bf16[2,512,2048]{2,1,0:T(8,128)(2,1)}) %all-gather.18.cloned.1.call-update) | async-done | bytes 4194320 | tf_op jit(solution)/shard_map/all_gather | solution.py:36
  633.9 8.2 convolution_convert_fusion.1
  642.1 0.0 all-gather.22.cloned.1.call-start
  642.1 41.7 %all-gather.20.cloned.1.call-done = bf16[2,704,2048]{2,1,0:T(8,128)(2,1)} async-done(((bf16[2,704,512]{2,1,0:T(8,128)(2,1)}), bf16[2,704,2048]{2,1,0:T(8,128)(2,1)}) %all-gather.20.cloned.1.call-update) | async-done | bytes 5767184 | tf_op jit(solution)/shard_map/all_gather | solution.py:45
  683.8 9.7 fusion.2
  693.5 0.0 all-gather.22.cloned.1.call-update
  693.6 0.3 reduce-scatter.8.cloned.1.call-start
  693.8 43.3 %all-gather.22.cloned.1.call-done = bf16[2,704,2048]{2,1,0:T(8,128)(2,1)} async-done(((bf16[2,704,512]{2,1,0:T(8,128)(2,1)}), bf16[2,704,2048]{2,1,0:T(8,128)(2,1)}) %all-gather.22.cloned.1.call-update) | async-done | bytes 5767184 | tf_op jit(solution)/shard_map/all_gather | solution.py:29
  737.1 9.9 fusion.5
  747.0 0.0 reduce-scatter.8.cloned.1.call-update
  747.0 0.0 all-gather.24.cloned.1.call-start
  747.1 147.9 %reduce-scatter.8.cloned.1.call-done = f32[2,512,256]{2,1,0:T(8,128)} async-done(((f32[2,512,2048]{2,1,0:T(8,128)}), f32[2,512,256]{2,1,0:T(8,128)}) %reduce-scatter.8.cloned.1.call-update) | async-done | bytes 1048592 | tf_op jit(solution)/shard_map/reduce_scatter | solution.py:33
  895.0 2.1 convert_element_type.45
  897.1 0.0 all-gather.24.cloned.1.call-update
  897.1 0.0 all-gather.26.cloned.1.call-start
  897.2 74.3 %all-gather.24.cloned.1.call-done = bf16[2,512,2048]{2,1,0:T(8,128)(2,1)} async-done(((bf16[2,512,256]{2,1,0:T(8,128)(2,1)}), bf16[2,512,2048]{2,1,0:T(8,128)(2,1)}) %all-gather.24.cloned.1.call-update) | async-done | bytes 4194320 | tf_op jit(solution)/shard_map/all_gather | solution.py:36
  971.4 8.2 convolution_convert_fusion
  979.6 41.7 %all-gather.26.cloned.1.call-done = bf16[2,704,2048]{2,1,0:T(8,128)(2,1)} async-done(((bf16[2,704,512]{2,1,0:T(8,128)(2,1)}), bf16[2,704,2048]{2,1,0:T(8,128)(2,1)}) %all-gather.26.cloned.1.call-update) | async-done | bytes 5767184 | tf_op jit(solution)/shard_map/all_gather | solution.py:45
  1021.3 11.6 %broadcast_multiply_fusion = (f32[2,704,512]{2,1,0:T(8,128)}, f32[2,704,512]{2,1,0:T(8,128)}) fusion(f32[2,704,512]{2,1,0:T(8,128)S(1)} %copy-done.1, bf16[2,704,2048]{2,1,0:T(8,128)(2,1)} %all-gather.26.cloned.1.call-done, bf16[2,512,2048]{2,1,0:T(8,128)(2,1)} %all-gather.24.cloned.1.call-done, bf16[2,704,512]{2,1,0:T(8,128)(2,1)} %convolution_convert_fusion, ...), kind=kOutput, calls=%fused_computation.9 | convolution fusion | flops 2959998976 | bytes 22937600 | tf_op jit(solution)/shard_map/prk,pjk->prj/dot_general | solution.py:43
  (10 shorter events, 0.1 us)
Async XLA Ops:
  7.2 51.8 %all-gather.10.cloned.1.call-start = ((), (), s32[]{:S(2)}) async-start(), calls=%async_computation.3 | async-start | bytes 7208960 | tf_op jit(solution)/shard_map/all_gather | solution.py:29
  12.7 204.2 %reduce-scatter.4.cloned.1.call-start = ((), (), s32[]{:S(2)}) async-start(), calls=%async_computation.4 | async-start | bytes 9437184 | tf_op jit(solution)/shard_map/reduce_scatter | solution.py:33
  68.9 226.3 %all-gather.12.cloned.1.call-start = ((), (), s32[]{:S(2)}) async-start(), calls=%async_computation.5 | async-start | bytes 4718592 | tf_op jit(solution)/shard_map/all_gather | solution.py:36
  219.5 125.9 %all-gather.14.cloned.1.call-start = ((), (), s32[]{:S(2)}) async-start(), calls=%async_computation.6 | async-start | bytes 7208960 | tf_op jit(solution)/shard_map/all_gather | solution.py:45
  295.2 50.1 %copy-start = (f32[2,704,512]{2,1,0:T(8,128)S(1)}, f32[2,704,512]{2,1,0:T(8,128)}, u32[]{:S(2)}) copy-start(f32[2,704,512]{2,1,0:T(8,128)} %param.5) | copy-start | bytes 8650756
  303.6 96.0 %all-gather.16.cloned.1.call-start = ((), (), s32[]{:S(2)}) async-start(), calls=%async_computation.7 | async-start | bytes 7208960 | tf_op jit(solution)/shard_map/all_gather | solution.py:29
  356.0 201.4 %reduce-scatter.6.cloned.1.call-start = ((), (), s32[]{:S(2)}) async-start(), calls=%async_computation.8 | async-start | bytes 9437184 | tf_op jit(solution)/shard_map/reduce_scatter | solution.py:33
  409.5 224.4 %all-gather.18.cloned.1.call-start = ((), (), s32[]{:S(2)}) async-start(), calls=%async_computation.9 | async-start | bytes 4718592 | tf_op jit(solution)/shard_map/all_gather | solution.py:36
  559.6 124.2 %copy-start.2 = (f32[2,704,512]{2,1,0:T(8,128)S(1)}, f32[2,704,512]{2,1,0:T(8,128)}, u32[]{:S(2)}) copy-start(f32[2,704,512]{2,1,0:T(8,128)} %get-tuple-element.14) | copy-start | bytes 8650756
  559.6 124.2 %all-gather.20.cloned.1.call-start = ((), (), s32[]{:S(2)}) async-start(), calls=%async_computation.10 | async-start | bytes 7208960 | tf_op jit(solution)/shard_map/all_gather | solution.py:45
  642.1 95.0 %all-gather.22.cloned.1.call-start = ((), (), s32[]{:S(2)}) async-start(), calls=%async_computation.11 | async-start | bytes 7208960 | tf_op jit(solution)/shard_map/all_gather | solution.py:29
  693.6 201.4 %reduce-scatter.8.cloned.1.call-start = ((), (), s32[]{:S(2)}) async-start(), calls=%async_computation.12 | async-start | bytes 9437184 | tf_op jit(solution)/shard_map/reduce_scatter | solution.py:33
  747.0 224.4 %all-gather.24.cloned.1.call-start = ((), (), s32[]{:S(2)}) async-start(), calls=%async_computation.13 | async-start | bytes 4718592 | tf_op jit(solution)/shard_map/all_gather | solution.py:36
  897.1 124.2 %copy-start.1 = (f32[2,704,512]{2,1,0:T(8,128)S(1)}, f32[2,704,512]{2,1,0:T(8,128)}, u32[]{:S(2)}) copy-start(f32[2,704,512]{2,1,0:T(8,128)} %param.3) | copy-start | bytes 8650756
  897.1 124.2 %all-gather.26.cloned.1.call-start = ((), (), s32[]{:S(2)}) async-start(), calls=%async_computation.14 | async-start | bytes 7208960 | tf_op jit(solution)/shard_map/all_gather | solution.py:45
Sparse Core Ops, SparseCore 0:
  12.9 46.0 all-gather.9
  69.1 147.8 reduce-scatter.3
  219.6 75.6 all-gather.11
  303.7 41.5 all-gather.13
  356.2 43.3 all-gather.15
  409.6 147.8 reduce-scatter.5
  560.1 73.7 all-gather.17
  642.2 41.5 all-gather.19
  693.7 43.3 all-gather.21
  747.1 147.8 reduce-scatter.7
  897.6 73.7 all-gather.23
  979.7 41.5 all-gather.25
where the time goes:
time: 1040 us
  waiting for transfers between devices  883 us (85%)
  matrix products  86.3 us (8%)
  blocking collectives  42.7 us (4%)
  between operations  14.2 us (1%)
  other arithmetic  12.2 us (1%)
    reduce_scatter x3, waiting for transfers between devices, per_device(): lax.psum_scatter(partial_value, 'fs', scatter_dimension=2, tiled=True)  444 us
    all_gather x3, waiting for transfers between devices, per_device(): lax.all_gather(gram_share.astype(jnp.bfloat16), 'fs', axis=2, tiled=True)  182 us
    all_gather x3, waiting for transfers between devices, per_device(): row_whole = lax.all_gather(plain, 'tp', axis=2, tiled=True)  133 us
    all_gather x3, waiting for transfers between devices, per_device(): lax.all_gather(cubed, 'tp', axis=2, tiled=True)  125 us
    psum x1, blocking collectives, per_device(): lax.psum(jnp.sum(gram_share * gram_share, axis=(1, 2)), ('fs', 'tp'))  42.7 us
    dot_general x3, matrix products, per_device(): jnp.einsum('prk,pjk->prj', lax.all_gather(cubed, 'tp', axis=2, tiled=True...  32 us
    dot_general x3, matrix products, per_device(): jnp.einsum('prj,prk->pjk', plain, row_whole, preferred_element_type=jnp.f...  29.7 us
    dot_general x3, matrix products, per_device(): jnp.einsum('prk,pjk->prj', row_whole, gram_bf, preferred_element_type=jnp...  24.6 us
  transfers between devices with their start and end apart: 12, of which 12 were waited for; matrix products, arithmetic and copies ran while one was open for 0% of the time, Pallas kernels for 0%

commit v1 on v0

v1 whole, which is shorter than its diff:
```python
import functools
import math

import jax
import jax.numpy as jnp
from jax import lax
from jax.experimental import pallas as pl
from jax.experimental.pallas import tpu as pltpu
from jax.sharding import Mesh, PartitionSpec as P

MOMENTUM_DECAY = 0.95
FIRST_COEF = 3.4445
SECOND_COEF = -4.775
THIRD_COEF = 2.0315
LEARN_RATE = 0.02
WEIGHT_DECAY = 0.1
EPSILON = 1e-07
STEP_SCALE = 0.2
NORM_SAFETY = 1.8
ITERS = 3

BLOCKS = 8
KEPT = BLOCKS // 2 + 1


def mm(a, b):
    return jnp.dot(a, b, preferred_element_type=jnp.float32)


def polar_kernel(scale_ref, wedge_ref, rows_ref, out_ref, gram, poly, half, wide):
    width = gram.shape[0]
    size = width // BLOCKS
    for i in range(BLOCKS):
        for k in range(KEPT):
            j = (i + k) % BLOCKS
            block = wedge_ref[i, :, k * size : (k + 1) * size]
            gram[i * size : (i + 1) * size, j * size : (j + 1) * size] = block
            if 0 < k < KEPT - 1:
                gram[j * size : (j + 1) * size, i * size : (i + 1) * size] = block.T

    ratio = scale_ref[0]
    square = scale_ref[1]
    tile = min(512, width)
    per_row = width // tile

    def over_tiles(body):
        def step(t, carry):
            i, j = t // per_row, t % per_row
            body(pl.ds(pl.multiple_of(i * tile, tile), tile), pl.ds(pl.multiple_of(j * tile, tile), tile))
            return carry

        lax.fori_loop(0, per_row * per_row, step, 0)

    for step in range(ITERS):
        unit = square if step == 0 else 1.0

        def to_poly(r, c):
            product = mm(gram[r, :], gram[:, c])
            mix = SECOND_COEF * gram[r, c].astype(jnp.float32) + (THIRD_COEF * unit) * product
            poly[r, c] = (unit * mix).astype(jnp.bfloat16)

        over_tiles(to_poly)

        def to_rows(t, carry):
            c = pl.ds(pl.multiple_of(t * tile, tile), tile)
            if step == 0:
                held = rows_ref[:, c].astype(jnp.float32)
                fresh = ratio * (FIRST_COEF * held + mm(rows_ref[...], poly[:, c]))
            else:
                fresh = FIRST_COEF * wide[:, c] + mm(out_ref[...], poly[:, c])
            wide[:, c] = fresh
            return carry

        lax.fori_loop(0, per_row, to_rows, 0)
        out_ref[...] = wide[...].astype(jnp.bfloat16)

        if step < ITERS - 1:

            def to_half(r, c):
                product = mm(gram[r, :], poly[:, c])
                half[r, c] = (unit * (FIRST_COEF * gram[r, c].astype(jnp.float32) + product)).astype(jnp.bfloat16)

            over_tiles(to_half)

            def to_gram(r, c):
                product = mm(half[r, :], poly[:, c])
                gram[r, c] = (FIRST_COEF * half[r, c].astype(jnp.float32) + product).astype(jnp.bfloat16)

            over_tiles(to_gram)


def polar(scales, wedge, rows):
    width = rows.shape[1]
    vmem = pl.BlockSpec(memory_space=pltpu.VMEM)
    return pl.pallas_call(
        polar_kernel,
        out_shape=jax.ShapeDtypeStruct(rows.shape, jnp.bfloat16),
        in_specs=[pl.BlockSpec(memory_space=pltpu.SMEM), vmem, vmem],
        out_specs=vmem,
        scratch_shapes=[
            pltpu.VMEM((width, width), jnp.bfloat16),
            pltpu.VMEM((width, width), jnp.bfloat16),
            pltpu.VMEM((width, width), jnp.bfloat16),
            pltpu.VMEM(rows.shape, jnp.float32),
        ],
        compiler_params=pltpu.CompilerParams(vmem_limit_bytes=56 * 1024 * 1024),
    )(scales, wedge, rows)


def per_device(subs, weights, momentum, gradients):
    mats, deep, narrow = gradients.shape
    width = narrow * mats * subs
    part = deep // subs
    new_momentum = MOMENTUM_DECAY * momentum + gradients
    plain = (gradients + MOMENTUM_DECAY * new_momentum).astype(jnp.bfloat16)

    pieces = plain.reshape(mats * subs, part, narrow)
    pieces = lax.all_to_all(pieces, ("mat", "sub"), 0, 0, tiled=True)
    rows = pieces.transpose(1, 0, 2).reshape(part, width)
    whole = lax.all_gather(rows, "sub", axis=0, tiled=True)

    size = width // BLOCKS
    own = BLOCKS // subs
    start = lax.axis_index("sub") * (own * size)
    turned = lax.dynamic_slice_in_dim(jnp.concatenate([whole, whole], axis=1), start, width, axis=1)
    partial_value = jnp.stack(
        [
            lax.dot_general(
                turned[:, b * size : (b + 1) * size],
                turned[:, b * size : (b + KEPT) * size],
                (((0,), (0,)), ((), ())),
                preferred_element_type=jnp.float32,
            ).astype(jnp.bfloat16)
            for b in range(own)
        ]
    )
    share = lax.psum_scatter(partial_value, "fs", scatter_dimension=1, tiled=True)
    wedge = lax.all_gather(share, "fs", axis=1, tiled=True)
    wedge = lax.all_gather(wedge, "sub", axis=0, tiled=True)

    by_block = jnp.sum(jnp.square(wedge.astype(jnp.float32)).reshape(BLOCKS * size, KEPT, size), axis=(0, 2))
    squares = 2.0 * jnp.sum(by_block) - by_block[0] - by_block[KEPT - 1]
    ratio = 1.0 / (NORM_SAFETY * jnp.sqrt(jnp.sqrt(squares / width)) + EPSILON)
    rows = polar(jnp.stack([ratio, ratio * ratio]), wedge, rows)

    pieces = rows.reshape(part, mats * subs, narrow).transpose(1, 0, 2)
    pieces = lax.all_to_all(pieces, ("mat", "sub"), 0, 0, tiled=True)
    iterate = pieces.reshape(mats, deep, narrow).astype(jnp.float32)
    deepest = deep * lax.axis_size("fs")
    update = STEP_SCALE * math.sqrt(max(deepest, width)) * iterate
    new_weights = weights * (1.0 - LEARN_RATE * WEIGHT_DECAY) - LEARN_RATE * update
    return (new_weights, new_momentum, update)


def solution(mesh):
    depth, tp = mesh.devices.shape
    mats = 2
    subs = tp // mats
    fine = Mesh(mesh.devices.reshape(depth, mats, subs), ("fs", "mat", "sub"))
    spec = P(None, "fs", ("mat", "sub"))
    return jax.shard_map(
        functools.partial(per_device, subs),
        mesh=fine,
        in_specs=(spec, spec, spec),
        out_specs=(spec, spec, spec),
        check_vma=False,
    )
```

time: 1040 us -> 403 us (0.39)
  waiting for transfers between devices: 883 us -> 155 us
  Pallas kernels: 0 us -> 159 us
  matrix products: 86.3 us -> 2.84 us
    reduce_scatter x3 -> x1, waiting for transfers between devices: 444 us -> 72.3 us  [per_device(): lax.psum_scatter(partial_value, 'fs', scatter_dimension=1, tiled=True)]
    all_gather x9 -> x3, waiting for transfers between devices: 439 us -> 82.8 us  [the longest x1 55.5 us: per_device(): wedge = lax.all_gather(share, 'fs', axis=1, tiled=True)]
    pallas_call x0 -> x1, Pallas kernels: none -> 159 us  [polar(): pl.pallas_call(polar_kernel, out_shape=jax.ShapeDtypeStruct(rows.shape, j...]
    dot_general x9 -> x4, matrix products: 86.3 us -> 2.84 us  [per_device(): lax.dot_general(turned[:, b * size:(b + 1) * size], turned[:, b * size:(b...]
    all_to_all x0 -> x2, blocking collectives: none -> 44.2 us  [per_device(): pieces = lax.all_to_all(pieces, ('mat', 'sub'), 0, 0, tiled=True)]
    psum x1 -> x0, blocking collectives: 42.7 us -> none  [per_device(): lax.psum(jnp.sum(gram_share * gram_share, axis=(1, 2)), ('fs', 'tp'))]
  transfers between devices with their start and end apart: 12 -> 4, of which waited for: 12 -> 4; matrix products, arithmetic and copies ran while one was open for 0% -> 0% of each run, Pallas kernels for 0% -> 0%
where the time goes in v1:
time: 403 us; the launch traced here: 402 us
  Pallas kernels  159 us (39%)
  waiting for transfers between devices  155 us (38%)
  blocking collectives  44.2 us (11%)
  other arithmetic  21.4 us (5%)
  between operations  15.8 us (4%)
    pallas_call x1, Pallas kernels, polar(): pl.pallas_call(polar_kernel, out_shape=jax.ShapeDtypeStruct(rows.shape, j...  159 us
    reduce_scatter x1, waiting for transfers between devices, per_device(): lax.psum_scatter(partial_value, 'fs', scatter_dimension=1, tiled=True)  72.3 us
    all_gather x1, waiting for transfers between devices, per_device(): wedge = lax.all_gather(share, 'fs', axis=1, tiled=True)  55.5 us
    all_to_all x2, blocking collectives, per_device(): pieces = lax.all_to_all(pieces, ('mat', 'sub'), 0, 0, tiled=True)  44.2 us
    all_gather x1, waiting for transfers between devices, per_device(): wedge = lax.all_gather(wedge, 'sub', axis=0, tiled=True)  15.2 us
    all_gather x1, waiting for transfers between devices, per_device(): whole = lax.all_gather(rows, 'sub', axis=0, tiled=True)  12.1 us
  transfers between devices with their start and end apart: 4, of which 4 were waited for; matrix products, arithmetic and copies ran while one was open for 0% of the time, Pallas kernels for 0%

profile of v1, /device:TPU:0, one launch (start us, length us, event | category | flops | bytes accessed | tf_op | source)
XLA Modules:
  0.0 402.4 jit_solution(1321894217955101729)
XLA Ops:
  7.2 0.0 all-gather.4.cloned.1.call-start
  7.2 5.1 %add_convert_fusion = (bf16[2,704,512]{2,1,0:T(8,128)(2,1)S(1)}, f32[2,704,512]{2,1,0:T(8,128)}) fusion(f32[2,704,512]{2,1,0:T(8,128)} %param.5, f32[2,704,512]{2,1,0:T(8,128)} %param.4), kind=kLoop, calls=%fused_computation.9 | loop fusion | flops 3604480 | bytes 10092544 | tf_op jit(solution)/shard_map/convert_element_type | solution.py:115
  12.3 22.7 %all_to_all.10 = bf16[4,352,512]{2,1,0:T(8,128)(2,1)S(1)} all-to-all(bf16[4,352,512]{2,1,0:T(8,128)(2,1)S(1)} %bitcast.30), channel_id=1, replica_groups=mesh['fs'=8,'mat'=2,'sub'=2] {'mat','sub'}, dimensions={0} | all-to-all | bytes 2883584 | tf_op jit(solution)/shard_map/all_to_all | solution.py:118
  35.0 1.3 copy.14
  36.3 0.0 all-gather.4.cloned.1.call-update
  36.3 0.0 reduce-scatter.2.cloned.1.call-start
  36.3 12.1 %all-gather.4.cloned.1.call-done = bf16[704,2048]{1,0:T(8,128)(2,1)} async-done(((bf16[352,2048]{1,0:T(8,128)(2,1)}), bf16[704,2048]{1,0:T(8,128)(2,1)}) %all-gather.4.cloned.1.call-update) | async-done | bytes 2883600 | tf_op jit(solution)/shard_map/all_gather | solution.py:120
  48.5 3.3 fusion.2
  51.7 0.7 fusion.5
  52.5 0.7 fusion.3
  53.2 0.7 fusion.4
  53.9 0.7 fusion.6
  54.6 1.8 pad_maximum_fusion
  56.4 0.0 reduce-scatter.2.cloned.1.call-update
  56.5 0.0 all-gather.6.cloned.1.call-start
  56.5 72.3 %reduce-scatter.2.cloned.1.call-done = bf16[4,32,1280]{2,1,0:T(8,128)(2,1)} async-done(((bf16[4,256,1280]{2,1,0:T(8,128)(2,1)}), bf16[4,32,1280]{2,1,0:T(8,128)(2,1)}) %reduce-scatter.2.cloned.1.call-update) | async-done | bytes 327696 | tf_op jit(solution)/shard_map/reduce_scatter | solution.py:137
  128.8 0.0 all-gather.6.cloned.1.call-update
  128.8 0.2 all-gather.8.cloned.1.call-start
  129.0 55.5 %all-gather.6.cloned.1.call-done = bf16[4,256,1280]{2,1,0:T(8,128)(2,1)} async-done(((bf16[4,32,1280]{2,1,0:T(8,128)(2,1)}), bf16[4,256,1280]{2,1,0:T(8,128)(2,1)}) %all-gather.6.cloned.1.call-update) | async-done | bytes 2621456 | tf_op jit(solution)/shard_map/all_gather | solution.py:138
  184.5 0.0 all-gather.8.cloned.1.call-update
  184.6 15.2 %all-gather.8.cloned.1.call-done.wedge_ref = bf16[8,256,1280]{2,1,0:T(8,128)(2,1)} async-done(((bf16[4,256,1280]{2,1,0:T(8,128)(2,1)}), bf16[8,256,1280]{2,1,0:T(8,128)(2,1)}) %all-gather.8.cloned.1.call-update) | async-done | bytes 5242896 | tf_op jit(solution)/shard_map/all_gather | solution.py:139
  199.8 5.9 %fusion = (f32[1280]{0:T(1024)S(1)}, f32[]{:T(128)}) fusion(bf16[8,256,1280]{2,1,0:T(8,128)(2,1)} %all-gather.8.cloned.1.call-done.wedge_ref), kind=kLoop, calls=%fused_computation.1 | loop fusion | flops 10484479 | bytes 5248004 | tf_op jit(solution)/shard_map/reduce_sum | solution.py:141
  205.7 0.1 reduce_sum.28
  205.8 0.6 fusion.15
  208.4 0.6 pad_maximum_fusion.1.scale_ref
  209.0 159.3 %shard_map.58 = bf16[352,2048]{1,0:T(8,128)(2,1)} custom-call(f32[2]{0:T(128)} %pad_maximum_fusion.1.scale_ref, bf16[8,256,1280]{2,1,0:T(8,128)(2,1)} %all-gather.8.cloned.1.call-done.wedge_ref, bf16[352,2048]{1,0:T(8,128)(2,1)} %bitcast.28), custom_call_target="tpu_custom_call" | custom-call | tf_op jit(solution)/shard_map/pallas_call | solution.py:95
  368.3 1.5 copy.16
  369.8 21.5 %all_to_all.11 = bf16[4,352,512]{2,1,0:T(8,128)(2,1)S(1)} all-to-all(bf16[4,352,512]{2,1,0:T(8,128)(2,1)S(1)} %bitcast.32), channel_id=1, replica_groups=mesh['fs'=8,'mat'=2,'sub'=2] {'mat','sub'}, dimensions={0} | all-to-all | bytes 2883584 | tf_op jit(solution)/shard_map/all_to_all | solution.py:147
  391.3 0.0 copy-start
  391.3 2.4 convert_multiply_fusion.1
  393.6 0.0 copy-done
  393.6 2.3 bitcast_subtract_fusion
  (1 shorter events, 0.0 us)
Async XLA Ops:
  7.2 41.3 %all-gather.4.cloned.1.call-start = ((), (), s32[]{:S(2)}) async-start(), calls=%async_computation.3 | async-start | bytes 4325376 | tf_op jit(solution)/shard_map/all_gather | solution.py:120
  36.3 92.5 %reduce-scatter.2.cloned.1.call-start = ((), (), s32[]{:S(2)}) async-start(), calls=%async_computation.4 | async-start | bytes 2949120 | tf_op jit(solution)/shard_map/reduce_scatter | solution.py:137
  56.5 128.1 %all-gather.6.cloned.1.call-start = ((), (), s32[]{:S(2)}) async-start(), calls=%async_computation.5 | async-start | bytes 2949120 | tf_op jit(solution)/shard_map/all_gather | solution.py:138
  128.8 71.0 %all-gather.8.cloned.1.call-start = ((), (), s32[]{:S(2)}) async-start(), calls=%async_computation.6 | async-start | bytes 7864320 | tf_op jit(solution)/shard_map/all_gather | solution.py:139
  391.3 2.4 copy-start
Sparse Core Ops, SparseCore 0:
  36.4 12.0 all-gather.3
  56.6 72.1 reduce-scatter.1
  131.0 53.5 all-gather.5
  185.9 13.7 all-gather.7

commit v2 on v1

v2 whole, which is shorter than its diff:
```python
import functools
import math

import jax
import jax.numpy as jnp
from jax import lax
from jax.experimental import pallas as pl
from jax.experimental.pallas import tpu as pltpu
from jax.sharding import Mesh, PartitionSpec as P

MOMENTUM_DECAY = 0.95
FIRST_COEF = 3.4445
SECOND_COEF = -4.775
THIRD_COEF = 2.0315
LEARN_RATE = 0.02
WEIGHT_DECAY = 0.1
EPSILON = 1e-07
STEP_SCALE = 0.2
NORM_SAFETY = 1.8
ITERS = 3

BLOCKS = 8
NEAR = BLOCKS // 2


def mm(a, b):
    return jnp.dot(a, b, preferred_element_type=jnp.float32)


def polar_kernel(subs, wedge_ref, rows_ref, out_ref, gram, poly, half, wide, tally):
    width = gram.shape[0]
    size = width // BLOCKS
    own = BLOCKS // subs
    per_sub = wedge_ref.shape[0] // subs

    def place(at, i, j, weight):
        block = wedge_ref[at]
        r = pl.ds(pl.multiple_of(i * size, size), size)
        c = pl.ds(pl.multiple_of(j * size, size), size)
        gram[r, c] = block
        if weight > 1.0:
            gram[c, r] = block.T
        full = block.astype(jnp.float32)
        tally[...] += weight * jnp.sum(full * full, axis=0, keepdims=True)

    tally[...] = jnp.zeros_like(tally)

    def place_row(i, carry):
        base = (i // own) * per_sub + (i % own) * NEAR
        for k in range(NEAR):
            place(base + k, i, (i + k) % BLOCKS, 1.0 if k == 0 else 2.0)
        return carry

    lax.fori_loop(0, BLOCKS, place_row, 0)
    for s in range(subs):
        for m in range(own // 2):
            i = s * own + m + (own // 2 if 2 * s >= subs else 0)
            place(s * per_sub + own * NEAR + m, i, (i + NEAR) % BLOCKS, 2.0)

    squares = jnp.sum(tally[...], axis=1, keepdims=True)
    first_ratio = 1.0 / (NORM_SAFETY * jnp.sqrt(jnp.sqrt(squares / width)) + EPSILON)
    wide[...] = rows_ref[...].astype(jnp.float32)
    out_ref[...] = rows_ref[...]
    tile = min(512, width)
    n = width // tile
    apart = n * (n - 1) // 2

    def spot(t):
        i = jnp.where(t < apart, t % n, t - apart)
        j = (i + jnp.where(t < apart, 1 + t // n, 0)) % n
        return pl.ds(pl.multiple_of(i * tile, tile), tile), pl.ds(pl.multiple_of(j * tile, tile), tile)

    def symmetric(target, tile_of):
        def step(t, carry):
            past_r, past_c = spot(jnp.maximum(t - 1, 0))
            target[past_c, past_r] = target[past_r, past_c].T
            r, c = spot(t)
            target[r, c] = tile_of(r, c).astype(jnp.bfloat16)
            return carry

        lax.fori_loop(0, apart + n, step, 0)

    def poly_and_rows(ratio):
        unit = ratio * ratio

        def poly_tile(r, c):
            return unit * (SECOND_COEF * gram[r, c].astype(jnp.float32) + (THIRD_COEF * unit) * mm(gram[r, :], gram[:, c]))

        symmetric(poly, poly_tile)

        def to_rows(t, carry):
            c = pl.ds(pl.multiple_of(t * tile, tile), tile)
            wide[:, c] = ratio * (FIRST_COEF * wide[:, c] + mm(out_ref[...], poly[:, c]))
            return carry

        lax.fori_loop(0, n, to_rows, 0)
        out_ref[...] = wide[...].astype(jnp.bfloat16)

    def full_step(step, carry):
        ratio = jnp.where(step == 0, first_ratio, 1.0)
        unit = ratio * ratio
        poly_and_rows(ratio)
        symmetric(half, lambda r, c: unit * (FIRST_COEF * gram[r, c].astype(jnp.float32) + mm(gram[r, :], poly[:, c])))
        symmetric(gram, lambda r, c: FIRST_COEF * half[r, c].astype(jnp.float32) + mm(half[r, :], poly[:, c]))
        return carry

    lax.fori_loop(0, ITERS - 1, full_step, 0)
    poly_and_rows(jnp.ones_like(first_ratio))


def polar(subs, wedge, rows):
    width = rows.shape[1]
    vmem = pl.BlockSpec(memory_space=pltpu.VMEM)
    return pl.pallas_call(
        functools.partial(polar_kernel, subs),
        out_shape=jax.ShapeDtypeStruct(rows.shape, jnp.bfloat16),
        in_specs=[vmem, vmem],
        out_specs=vmem,
        scratch_shapes=[
            pltpu.VMEM((width, width), jnp.bfloat16),
            pltpu.VMEM((width, width), jnp.bfloat16),
            pltpu.VMEM((width, width), jnp.bfloat16),
            pltpu.VMEM(rows.shape, jnp.float32),
            pltpu.VMEM((1, width // BLOCKS), jnp.float32),
        ],
        compiler_params=pltpu.CompilerParams(vmem_limit_bytes=56 * 1024 * 1024),
    )(wedge, rows)


def per_device(subs, weights, momentum, gradients):
    mats, deep, narrow = gradients.shape
    width = narrow * mats * subs
    part = deep // subs
    new_momentum = MOMENTUM_DECAY * momentum + gradients
    plain = (gradients + MOMENTUM_DECAY * new_momentum).astype(jnp.bfloat16)

    pieces = plain.reshape(mats * subs, part, narrow)
    pieces = lax.all_to_all(pieces, ("mat", "sub"), 0, 0, tiled=True)
    rows = pieces.transpose(1, 0, 2).reshape(part, width)
    whole = lax.all_gather(rows, "sub", axis=0, tiled=True)

    size = width // BLOCKS
    own = BLOCKS // subs
    sub = lax.axis_index("sub")
    start = sub * (own * size)
    turned = lax.dynamic_slice_in_dim(jnp.concatenate([whole, whole], axis=1), start, width, axis=1)

    def product(left, right):
        full = lax.dot_general(left, right, (((0,), (0,)), ((), ())), preferred_element_type=jnp.float32)
        full = full.astype(jnp.bfloat16)
        return [full[:, at : at + size] for at in range(0, full.shape[1], size)]

    blocks = []
    for b in range(own):
        blocks += product(turned[:, b * size : (b + 1) * size], turned[:, b * size : (b + NEAR) * size])
    far = jnp.where(2 * sub >= subs, (own // 2) * size, 0)
    for m in range(own // 2):
        left = lax.dynamic_slice_in_dim(turned, far + m * size, size, axis=1)
        right = lax.dynamic_slice_in_dim(turned, far + (m + NEAR) * size, size, axis=1)
        blocks += product(left, right)
    share = lax.psum_scatter(jnp.stack(blocks), "fs", scatter_dimension=1, tiled=True)
    wedge = lax.all_gather(share, "fs", axis=1, tiled=True)
    wedge = lax.all_gather(wedge, "sub", axis=0, tiled=True)
    rows = polar(subs, wedge, rows)

    pieces = rows.reshape(part, mats * subs, narrow).transpose(1, 0, 2)
    pieces = lax.all_to_all(pieces, ("mat", "sub"), 0, 0, tiled=True)
    iterate = pieces.reshape(mats, deep, narrow).astype(jnp.float32)
    deepest = deep * lax.axis_size("fs")
    update = STEP_SCALE * math.sqrt(max(deepest, width)) * iterate
    new_weights = weights * (1.0 - LEARN_RATE * WEIGHT_DECAY) - LEARN_RATE * update
    return (new_weights, new_momentum, update)


def solution(mesh):
    depth, tp = mesh.devices.shape
    mats = 2
    subs = tp // mats
    fine = Mesh(mesh.devices.reshape(depth, mats, subs), ("fs", "mat", "sub"))
    spec = P(None, "fs", ("mat", "sub"))
    return jax.shard_map(
        functools.partial(per_device, subs),
        mesh=fine,
        in_specs=(spec, spec, spec),
        out_specs=(spec, spec, spec),
        check_vma=False,
    )
```

time: 403 us -> 339 us (0.84)
  Pallas kernels: 159 us -> 108 us
  other arithmetic: 21.4 us -> 9.71 us
  local copies, waits for them, and re-layouts: 3.34 us -> 7.48 us
    pallas_call x1, Pallas kernels: 159 us -> 108 us  [polar(): pl.pallas_call(functools.partial(polar_kernel, subs), out_shape=jax.Shape...]
    reduce_sum x2 -> x0, other arithmetic: 6.01 us -> none  [per_device(): jnp.sum(jnp.square(wedge.astype(jnp.float32)).reshape(BLOCKS * size, KEPT...]
    unnamed x2 -> x23, local copies, waits for them, and re-layouts: 0.01 us -> 4.39 us
where the time goes in v2:
time: 339 us
  waiting for transfers between devices  151 us (45%)
  Pallas kernels  108 us (32%)
  blocking collectives  44.2 us (13%)
  between operations  14 us (4%)
  other arithmetic  9.71 us (3%)
  local copies, waits for them, and re-layouts  7.48 us (2%)
  matrix products  3.74 us (1%)
    pallas_call x1, Pallas kernels, polar(): pl.pallas_call(functools.partial(polar_kernel, subs), out_shape=jax.Shape...  108 us
    reduce_scatter x1, waiting for transfers between devices, per_device(): lax.psum_scatter(jnp.stack(blocks), 'fs', scatter_dimension=1, tiled=True)  71.4 us
    all_gather x1, waiting for transfers between devices, per_device(): wedge = lax.all_gather(share, 'fs', axis=1, tiled=True)  53.2 us
    all_to_all x2, blocking collectives, per_device(): pieces = lax.all_to_all(pieces, ('mat', 'sub'), 0, 0, tiled=True)  44.2 us
    all_gather x1, waiting for transfers between devices, per_device(): wedge = lax.all_gather(wedge, 'sub', axis=0, tiled=True)  14.4 us
    all_gather x1, waiting for transfers between devices, per_device(): whole = lax.all_gather(rows, 'sub', axis=0, tiled=True)  12.1 us
  transfers between devices with their start and end apart: 4, of which 4 were waited for; matrix products, arithmetic and copies ran while one was open for 0% of the time, Pallas kernels for 0%

profile of v2, /device:TPU:0, one launch (start us, length us, event | category | flops | bytes accessed | tf_op | source)
XLA Modules:
  0.0 338.8 jit_solution(3544072551823460262)
XLA Ops:
  7.2 0.0 all-gather.4.cloned.1.call-start
  7.2 5.1 %add_convert_fusion = (bf16[2,704,512]{2,1,0:T(8,128)(2,1)S(1)}, f32[2,704,512]{2,1,0:T(8,128)}) fusion(f32[2,704,512]{2,1,0:T(8,128)} %param.5, f32[2,704,512]{2,1,0:T(8,128)} %param.4), kind=kLoop, calls=%fused_computation.3 | loop fusion | flops 3604480 | bytes 10092544 | tf_op jit(solution)/shard_map/convert_element_type | solution.py:135
  12.3 22.7 %all_to_all.10 = bf16[4,352,512]{2,1,0:T(8,128)(2,1)S(1)} all-to-all(bf16[4,352,512]{2,1,0:T(8,128)(2,1)S(1)} %bitcast.90), channel_id=1, replica_groups=mesh['fs'=8,'mat'=2,'sub'=2] {'mat','sub'}, dimensions={0} | all-to-all | bytes 2883584 | tf_op jit(solution)/shard_map/all_to_all | solution.py:138
  35.0 1.3 copy.12
  36.3 0.0 all-gather.4.cloned.1.call-update
  36.3 0.0 reduce-scatter.2.cloned.1.call-start
  36.3 12.1 %all-gather.4.cloned.1.call-done = bf16[704,2048]{1,0:T(8,128)(2,1)} async-done(((bf16[352,2048]{1,0:T(8,128)(2,1)}), bf16[704,2048]{1,0:T(8,128)(2,1)}) %all-gather.4.cloned.1.call-update) | async-done | bytes 2883600 | tf_op jit(solution)/shard_map/all_gather | solution.py:140
  48.5 0.0 copy-start
  48.5 2.2 constant_dynamic-update-slice_fusion.1
  50.6 0.5 copy-done
  51.1 0.4 constant_dynamic-update-slice_fusion
  51.5 0.6 fusion.8
  52.2 0.6 fusion.11
  53.0 0.6 fusion.14
  53.7 0.6 fusion.17
  54.4 0.6 fusion.21
  55.1 0.6 fusion.23
  55.7 0.0 copy-start.2
  55.7 1.4 copy-done.2
  57.1 0.0 reduce-scatter.2.cloned.1.call-update
  57.1 0.0 all-gather.6.cloned.1.call-start
  57.2 71.4 %reduce-scatter.2.cloned.1.call-done = bf16[18,32,256]{2,1,0:T(8,128)(2,1)} async-done(((bf16[18,256,256]{2,1,0:T(8,128)(2,1)}), bf16[18,32,256]{2,1,0:T(8,128)(2,1)}) %reduce-scatter.2.cloned.1.call-update) | async-done | bytes 294928 | tf_op jit(solution)/shard_map/reduce_scatter | solution.py:161
  128.6 0.0 all-gather.6.cloned.1.call-update
  128.6 0.0 all-gather.8.cloned.1.call-start
  128.7 53.2 %all-gather.6.cloned.1.call-done = bf16[18,256,256]{2,1,0:T(8,128)(2,1)} async-done(((bf16[18,32,256]{2,1,0:T(8,128)(2,1)}), bf16[18,256,256]{2,1,0:T(8,128)(2,1)}) %all-gather.6.cloned.1.call-update) | async-done | bytes 2359312 | tf_op jit(solution)/shard_map/all_gather | solution.py:162
  181.8 0.0 all-gather.8.cloned.1.call-update
  181.8 14.4 %all-gather.8.cloned.1.call-done.wedge_ref = bf16[36,256,256]{2,1,0:T(8,128)(2,1)} async-done(((bf16[18,256,256]{2,1,0:T(8,128)(2,1)}), bf16[36,256,256]{2,1,0:T(8,128)(2,1)}) %all-gather.8.cloned.1.call-update) | async-done | bytes 4718608 | tf_op jit(solution)/shard_map/all_gather | solution.py:163
  196.2 108.5 %shard_map.58 = bf16[352,2048]{1,0:T(8,128)(2,1)} custom-call(bf16[36,256,256]{2,1,0:T(8,128)(2,1)} %all-gather.8.cloned.1.call-done.wedge_ref, bf16[352,2048]{1,0:T(8,128)(2,1)} %bitcast.88), custom_call_target="tpu_custom_call" | custom-call | tf_op jit(solution)/shard_map/pallas_call | solution.py:114
  304.7 1.5 copy.14
  306.2 21.5 %all_to_all.11 = bf16[4,352,512]{2,1,0:T(8,128)(2,1)S(1)} all-to-all(bf16[4,352,512]{2,1,0:T(8,128)(2,1)S(1)} %bitcast.92), channel_id=1, replica_groups=mesh['fs'=8,'mat'=2,'sub'=2] {'mat','sub'}, dimensions={0} | all-to-all | bytes 2883584 | tf_op jit(solution)/shard_map/all_to_all | solution.py:167
  327.6 0.0 copy-start.1
  327.6 2.4 convert_multiply_fusion
  330.0 0.0 copy-done.1
  330.0 2.3 bitcast_subtract_fusion
  (16 shorter events, 0.3 us)
Async XLA Ops:
  7.2 41.3 %all-gather.4.cloned.1.call-start = ((), (), s32[]{:S(2)}) async-start(), calls=%async_computation.3 | async-start | bytes 4325376 | tf_op jit(solution)/shard_map/all_gather | solution.py:140
  36.3 92.3 %reduce-scatter.2.cloned.1.call-start = ((), (), s32[]{:S(2)}) async-start(), calls=%async_computation.4 | async-start | bytes 2654208 | tf_op jit(solution)/shard_map/reduce_scatter | solution.py:161
  48.5 2.7 copy-start
  55.7 1.4 copy-start.2
  57.1 124.7 %all-gather.6.cloned.1.call-start = ((), (), s32[]{:S(2)}) async-start(), calls=%async_computation.5 | async-start | bytes 2654208 | tf_op jit(solution)/shard_map/all_gather | solution.py:162
  128.6 67.6 %all-gather.8.cloned.1.call-start = ((), (), s32[]{:S(2)}) async-start(), calls=%async_computation.6 | async-start | bytes 7077888 | tf_op jit(solution)/shard_map/all_gather | solution.py:163
  327.6 2.4 copy-start.1
Sparse Core Ops, SparseCore 0:
  36.4 12.0 all-gather.3
  57.3 71.2 reduce-scatter.1
  130.8 50.9 all-gather.5
  183.2 12.9 all-gather.7
